TPU v7x, 32 devices: a whole 2x2x4 slice. The times are simulated.
32 devices in a mesh: sp: 16 (over z, y, x), tp: 2 (over core).
Axes of the slice: x: 2, y: 2, z: 4, core: 2. Of those that a mesh axis runs over, the one named last changes fastest.
Arguments:
- latent: bfloat16 [4096, 2048], P(('sp', 'tp')), may hold values from -3 to 3
- context: bfloat16 [1024, 2048], P('sp'), may hold values from -6 to 6
- condition: float32 [2048], replicated, may hold values from -6 to 6
- ctx_cond: float32 [2048], replicated, may hold values from -6 to 6
- norm_gain: float32 [2048], replicated, may hold values from 0.1 to 1.9
- w_shift: bfloat16 [2048, 2048], P('sp', 'tp'), may hold values from -0.25 to 0.25
- w_scale: bfloat16 [2048, 2048], P('sp', 'tp'), may hold values from -0.25 to 0.25
- w_gate: bfloat16 [2048, 2048], P('sp', 'tp'), may hold values from -0.25 to 0.25
- w_query: bfloat16 [2048, 2048], P(None, 'tp'), may hold values from -0.125 to 0.125
- w_key: bfloat16 [2048, 2048], P(None, 'tp'), may hold values from -0.125 to 0.125
- w_value: bfloat16 [2048, 2048], P(None, 'tp'), may hold values from -0.125 to 0.125
- w_out: bfloat16 [2048, 2048], P('tp'), may hold values from -0.125 to 0.125
- rel_bias: float32 [16, 15, 31], replicated, may hold values from 2 to 250
Outputs:
- updated: bfloat16 [4096, 2048], P(('sp', 'tp'))
All inputs are finite; a program needn't handle non-finite values.
Results may differ from a plain program's by a relative error of at most 0.015.
Values may be sent and summed in bfloat16 or wider, within the bound.
A program may use at most 128 MiB of HBM per device.

v0:
```python
import jax
import jax.numpy as jnp
from jax import lax
from jax.sharding import PartitionSpec as P

HEADS = 16
HEAD_DIM = 128
GRID_W = 32
WIN_H = 8
WIN_W = 16
NORM_EPS = 1e-06
NEG_BIG = -1e30


def padded_2(cells, sides, width):
    for axis, dim in sides:
        count = lax.axis_size(axis)
        ends = count - 1
        head = lax.slice_in_dim(cells, 0, width, axis=dim)
        tail = lax.slice_in_dim(cells, cells.shape[dim] - width, cells.shape[dim], axis=dim)
        cells = jnp.concatenate(
            [
                lax.ppermute(tail, axis, [(i, (i + 1) % count) for i in range(ends)]),
                cells,
                lax.ppermute(head, axis, [((i + 1) % count, i) for i in range(ends)]),
            ],
            axis=dim,
        )
    return cells


def rms_mod(block, norm_gain, shifts, scales):
    block = block.astype(jnp.float32)
    normed = (
        block * lax.rsqrt(jnp.mean(block * block, axis=-1, keepdims=True) + NORM_EPS) * norm_gain
    )
    return (normed * (1.0 + scales) + shifts).astype(jnp.bfloat16)


def project(block, weights):
    return jnp.stack(
        [
            jnp.dot(block, weight, preferred_element_type=jnp.float32).astype(jnp.bfloat16)
            for weight in weights
        ]
    )


def on_device(
    latent,
    context,
    condition,
    ctx_cond,
    norm_gain,
    w_shift,
    w_scale,
    w_gate,
    w_query,
    w_key,
    w_value,
    w_out,
    rel_bias,
):
    tp_size = lax.axis_size("tp")
    sp_size = lax.axis_size("sp")
    head_dev = HEADS // tp_size
    head_cols = w_query.shape[1]
    model_width = w_query.shape[0]
    row_part = w_shift.shape[0]
    col_part = w_shift.shape[1]
    activated = jax.nn.silu(jnp.stack([condition, ctx_cond])).astype(jnp.bfloat16)
    act_rows = lax.dynamic_slice_in_dim(activated, lax.axis_index("sp") * row_part, row_part, 1)
    partial_value = jnp.concatenate(
        [
            jnp.dot(act_rows, w_shift, preferred_element_type=jnp.float32),
            jnp.dot(act_rows, w_scale, preferred_element_type=jnp.float32),
            jnp.dot(act_rows[:1], w_gate, preferred_element_type=jnp.float32),
        ],
        axis=0,
    )
    placed = lax.dynamic_update_slice_in_dim(
        jnp.zeros((5, model_width), jnp.float32), partial_value, lax.axis_index("tp") * col_part, 1
    )
    mod_vecs = lax.psum(placed, ("sp", "tp"))
    normed = rms_mod(latent, norm_gain, mod_vecs[0], mod_vecs[2])
    projected = project(lax.all_gather(normed, "tp", axis=0, tiled=True), (w_query, w_key, w_value))
    ctx_kv = lax.all_gather(
        project(rms_mod(context, norm_gain, mod_vecs[1], mod_vecs[3]), (w_key, w_value)),
        "sp",
        axis=1,
        tiled=True,
    )
    ctx_key3 = ctx_kv[0].reshape(-1, head_dev, HEAD_DIM)
    ctx_val3 = ctx_kv[1].reshape(-1, head_dev, HEAD_DIM)
    grid_rows = projected.shape[1] // GRID_W
    queries = projected[0].reshape(grid_rows, GRID_W, head_dev, HEAD_DIM)
    half_win = WIN_H // 2
    padded = padded_2(
        projected[1:].reshape(2, grid_rows, GRID_W, head_cols), (("sp", 1),), half_win
    )
    total_rows = grid_rows * sp_size
    first_row = lax.axis_index("sp") * grid_rows
    local_rows = jnp.arange(grid_rows, dtype=jnp.int32)
    starts = (
        jnp.clip(first_row + local_rows - half_win, 0, total_rows - WIN_H) - first_row + half_win
    )

    def take_window(start_row):
        return lax.dynamic_slice_in_dim(padded, start_row, WIN_H, 1)

    windows = jax.vmap(take_window)(starts)
    key_win = windows[:, 0].reshape(grid_rows, WIN_H, GRID_W, head_dev, HEAD_DIM)
    val_win = windows[:, 1].reshape(grid_rows, WIN_H, GRID_W, head_dev, HEAD_DIM)
    row_off = (
        starts[:, None]
        - half_win
        + jnp.arange(WIN_H, dtype=jnp.int32)[None, :]
        - local_rows[:, None]
        + WIN_H
        - 1
    )
    col_ids = jnp.arange(GRID_W, dtype=jnp.int32)
    col_start = jnp.clip(col_ids - WIN_W // 2, 0, GRID_W - WIN_W)
    col_in = (col_ids[None, :] >= col_start[:, None]) & (
        col_ids[None, :] < col_start[:, None] + WIN_W
    )
    col_off = jnp.clip(col_ids[None, :] - col_ids[:, None], 1 - WIN_W, WIN_W - 1) + WIN_W - 1
    col_hot = (col_off[:, :, None] == jnp.arange(2 * WIN_W - 1)[None, None, :]).astype(jnp.float32)
    row_hot = (row_off[:, :, None] == jnp.arange(2 * WIN_H - 1)[None, None, :]).astype(jnp.float32)
    bias_table = lax.dynamic_slice_in_dim(rel_bias, lax.axis_index("tp") * head_dev, head_dev, 0)
    col_table = jnp.einsum("hec,qwc->heqw", bias_table, col_hot, precision=lax.Precision.HIGHEST)
    bias_win = jnp.einsum("rke,heqw->rqhkw", row_hot, col_table, precision=lax.Precision.HIGHEST)
    inv_scale = HEAD_DIM ** (-0.5)
    scores_win = (
        jnp.einsum("rqhd,rkwhd->rqhkw", queries, key_win, preferred_element_type=jnp.float32)
        * inv_scale
        + bias_win
    )
    scores_win = jnp.where(col_in[None, :, None, None, :], scores_win, NEG_BIG)
    scores_win = scores_win.reshape(grid_rows, GRID_W, head_dev, WIN_H * GRID_W)
    scores_ctx = (
        jnp.einsum("rqhd,chd->rqhc", queries, ctx_key3, preferred_element_type=jnp.float32)
        * inv_scale
    )
    row_max = jnp.maximum(jnp.max(scores_win, axis=-1), jnp.max(scores_ctx, axis=-1))
    exp_win = jnp.exp(scores_win - row_max[..., None])
    exp_ctx = jnp.exp(scores_ctx - row_max[..., None])
    row_total = jnp.sum(exp_win, axis=-1) + jnp.sum(exp_ctx, axis=-1)
    probs_win = (exp_win / row_total[..., None]).astype(jnp.bfloat16)
    probs_win = probs_win.reshape(grid_rows, GRID_W, head_dev, WIN_H, GRID_W)
    probs_ctx = (exp_ctx / row_total[..., None]).astype(jnp.bfloat16)
    attended = jnp.einsum(
        "rqhkw,rkwhd->rqhd", probs_win, val_win, preferred_element_type=jnp.float32
    )
    attended = attended + jnp.einsum(
        "rqhc,chd->rqhd", probs_ctx, ctx_val3, preferred_element_type=jnp.float32
    )
    attended = attended.astype(jnp.bfloat16).reshape(grid_rows * GRID_W, head_cols)
    branch = lax.psum_scatter(
        jnp.dot(attended, w_out, preferred_element_type=jnp.float32).astype(jnp.bfloat16),
        "tp",
        scatter_dimension=0,
        tiled=True,
    ).astype(jnp.float32)
    return (latent.astype(jnp.float32) + mod_vecs[4] * branch).astype(jnp.bfloat16)


def solution(mesh):
    placed = (
        P(("sp", "tp"), None),
        P("sp", None),
        P(),
        P(),
        P(),
        P("sp", "tp"),
        P("sp", "tp"),
        P("sp", "tp"),
        P(None, "tp"),
        P(None, "tp"),
        P(None, "tp"),
        P("tp", None),
        P(),
    )
    return jax.shard_map(
        on_device, mesh=mesh, in_specs=placed, out_specs=P(("sp", "tp"), None), check_vma=False
    )
```

profile of v0, /device:TPU:0, one launch (start us, length us, event | category | flops | bytes accessed | tf_op | source)
XLA Modules:
  0.0 193.7 jit_solution(12751256618278326930)
XLA Ops:
  9.9 42.3 %psum.7 = f32[5,2048]{1,0:T(8,128)S(1)} all-reduce(f32[5,2048]{1,0:T(8,128)S(1)} %maximum_dynamic-update-slice_fusion), channel_id=1, replica_groups=mesh['sp'=16,'tp'=2] {'sp','tp'}, use_global_device_ids=true, to_apply=%region_0.1 | all-reduce | flops 10240 | bytes 81920 | tf_op jit(solution)/shard_map/psum | solution.py:84
  53.5 2.1 %fusion.39 = bf16[128,2048]{1,0:T(8,128)(2,1)} fusion(bf16[128,2048]{1,0:T(8,128)(2,1)} %param.13, f32[2048]{0:T(1024)S(1)} %bitcast.155, f32[2048]{0:T(1024)S(1)} %bitcast.156, f32[2048]{0:T(1024)} %param.17, f32[128]{0:T(128)S(1)} %add_rsqrt_fusion.1), kind=kLoop, calls=%fused_computation.46 | loop fusion | flops 1572864 | bytes 1073664 | tf_op jit(solution)/shard_map/convert_element_type | solution.py:37
  57.0 3.2 %fusion.33 = bf16[1,64,1024]{2,1,0:T(8,128)(2,1)S(1)} fusion(bf16[2048,1024]{1,0:T(8,128)(2,1)} %param.22, bf16[64,2048]{1,0:T(8,128)(2,1)} %param.14, f32[2048]{0:T(1024)S(1)} %bitcast.150, f32[2048]{0:T(1024)S(1)} %bitcast.152, f32[2048]{0:T(1024)} %param.17, f32[64]{0:T(128)S(1)} %add_rsqrt_fusion), kind=kOutput, calls=%fused_computation.40 | convolution fusion | flops 269287424 | bytes 4612352 | tf_op jit(solution)/shard_map/dot_general | solution.py:43
  62.1 1.4 fusion.51
  63.5 5.6 %fusion.12 = f32[8,32,32,8,8]{2,4,3,1,0:T(8,128)} fusion(f32[8,15,32,32]{3,1,2,0:T(8,128)S(1)} %fusion.51, s32[8,8]{1,0:T(8,128)S(1)} %subtract_add_fusion), kind=kOutput, calls=%fused_computation.21 | convolution fusion | flops 94372800 | bytes 2588928 | tf_op jit(solution)/shard_map/rke,heqw->rqhkw/dot_general | solution.py:132
  69.2 9.3 %copy.59 = f32[8,32,32,8,8]{1,2,4,0,3:T(8,128)} copy(f32[8,32,32,8,8]{2,4,3,1,0:T(8,128)} %fusion.12) | data formatting | bytes 4194304 | tf_op jit(solution)/shard_map/rke,heqw->rqhkw/dot_general | solution.py:132
  78.5 3.9 %convolution_convert_fusion.2 = bf16[256,1024]{1,0:T(8,128)(2,1)S(1)} fusion(bf16[256,2048]{1,0:T(8,128)(2,1)} %all-gather.3.cloned.1.call-done, bf16[2048,1024]{1,0:T(8,128)(2,1)} %param.23), kind=kOutput, calls=%fused_computation.35 | convolution fusion | flops 1074003968 | bytes 5767168 | tf_op jit(solution)/shard_map/dot_general | solution.py:43
  83.9 4.2 %collective-permute-start = (bf16[2,4,32,1024]{3,2,0,1:T(8,128)(2,1)S(1)}, bf16[2,4,32,1024]{3,2,0,1:T(8,128)(2,1)S(1)}, u32[]{:S(2)}, u32[]{:S(2)}) collective-permute-start(bf16[2,4,32,1024]{3,2,0,1:T(8,128)(2,1)S(1)} %get-tuple-element.9), channel_id=1, source_target_pairs={{0,2},{2,4},{4,6},{6,8},{8,10},{10,12},{12,14},{14,16},{16,18},{18... | collective-permute-start | bytes 1572872 | tf_op jit(solution)/shard_map/ppermute | solution.py:23
  88.2 1.3 collective-permute-start.1
  91.0 25.2 %collective-permute-done = bf16[2,4,32,1024]{3,2,0,1:T(8,128)(2,1)S(1)} collective-permute-done((bf16[2,4,32,1024]{3,2,0,1:T(8,128)(2,1)S(1)}, bf16[2,4,32,1024]{3,2,0,1:T(8,128)(2,1)S(1)}, u32[]{:S(2)}, u32[]{:S(2)}) %collective-permute-start) | collective-permute-done | bytes 524320 | tf_op jit(solution)/shard_map/ppermute | solution.py:23
  116.2 1.9 collective-permute-done.1
  118.4 4.9 %gather_fusion = bf16[8,2,8,32,1024]{4,3,1,2,0:T(8,128)(2,1)} fusion(bf16[2,16,32,1024]{3,2,0,1:T(8,128)(2,1)S(1)} %pad_maximum_fusion, s32[8]{0:T(128)S(1)} %shift-left_bitcast_fusion), kind=kCustom, calls=%fused_computation | custom fusion | bytes 16777344 | tf_op jit(solution)/shard_map/vmap()/gather | solution.py:109
  123.3 4.0 %fusion.66 = (bf16[8,1,8,32,1024]{4,3,1,2,0:T(8,128)(2,1)S(1)}, bf16[8,1,8,32,1024]{4,3,1,2,0:T(8,128)(2,1)S(1)}) fusion(bf16[8,2,8,32,1024]{4,3,1,2,0:T(8,128)(2,1)} %gather_fusion), kind=kLoop, calls=%fused_computation.99 | loop fusion | bytes 16777216 | tf_op jit(solution)/shard_map/slice | solution.py:113
  128.4 3.3 %copy.80 = bf16[256,8,8,128]{3,2,1,0:T(8,128)(2,1)} copy(bf16[256,8,8,128]{3,1,2,0:T(8,128)(2,1)S(1)} %bitcast.137) | data formatting | bytes 8388608
  132.9 4.3 %fusion.68 = (f32[8,32,8]{1,2,0:T(8,128)S(1)}, f32[8,32,8,8,32]{1,4,3,2,0:T(8,128)}) fusion(f32[8,32,32,8,8]{1,2,4,0,3:T(8,128)S(1)} %bitcast.133, bf16[8,32,8,128,1]{3,2,1,0,4:T(8,128)(2,1)S(1)} %bitcast_bitcast_fusion, bf16[8,8,32,8,128]{4,3,2,1,0:T(8,128)(2,1)S(1)} %bitcast.136, pred[32,32]{0,1:T(8,128)(4,1)S(1)} %fusion.57), kind=kOutput, calls=%fused_computation.101 | convolution fusion | flops 136312832 | bytes 8922112 | tf_op jit(solution)/shard_map/rqhd,rkwhd->rqhkw/dot_general | solution.py:135
  137.2 19.0 %all-gather.5.cloned.1.call-done = bf16[2,1024,1024]{2,1,0:T(8,128)(2,1)} async-done(((bf16[2,64,1024]{2,1,0:T(8,128)(2,1)}), bf16[2,1024,1024]{2,1,0:T(8,128)(2,1)}) %all-gather.5.cloned.1.call-update) | async-done | bytes 4194320 | tf_op jit(solution)/shard_map/all_gather | solution.py:87
  156.2 3.2 %slice_bitcast_fusion = (bf16[128,8,8,128]{3,1,2,0:T(8,128)(2,1)S(1)}, bf16[128,8,8,128]{3,1,2,0:T(8,128)(2,1)S(1)}) fusion(bf16[2,1024,1024]{2,1,0:T(8,128)(2,1)} %all-gather.5.cloned.1.call-done), kind=kLoop, calls=%fused_computation.18 | loop fusion | bytes 8388608
  162.0 1.9 fusion.3
  164.9 2.0 %fusion.2 = f32[8,32,8]{1,2,0:T(8,128)S(1)} fusion(f32[8,32,8,8,32]{1,4,3,2,0:T(8,128)S(1)} %bitcast.135, f32[8,32,8]{1,2,0:T(8,128)S(1)} %copy_maximum_fusion), kind=kLoop, calls=%fused_computation.9 | loop fusion | flops 1046528 | bytes 2113536 | tf_op jit(solution)/shard_map/reduce_sum | solution.py:148
  167.6 3.3 %fusion.21 = f32[8,32,8,128]{3,1,2,0:T(8,128)S(1)} fusion(bf16[1024,8,128]{2,1,0:T(8,128)(2,1)S(1)} %bitcast.143, f32[8,32,8]{1,0,2:T(8,128)S(1)} %copy.67, f32[8,32,8]{1,0,2:T(8,128)S(1)} %copy.63, f32[8,1024,256]{1,2,0:S(1)} %fusion.16), kind=kOutput, calls=%fused_computation.31 | convolution fusion | flops 545259520 | bytes 11550720 | tf_op jit(solution)/shard_map/rqhc,chd->rqhd/dot_general | solution.py:155
  170.9 2.3 %fusion.29 = bf16[8,32,8,128]{3,1,2,0:T(8,128)(2,1)S(1)} fusion(f32[8,32,8,128]{3,1,2,0:T(8,128)S(1)} %fusion.21, f32[8,32,8,8,32]{1,4,3,2,0:T(8,128)S(1)} %bitcast.135, f32[8,32,8]{1,2,0:T(8,128)S(1)} %copy_add_fusion, f32[8,32,8]{1,2,0:T(8,128)S(1)} %copy_maximum_fusion, bf16[8,8,32,8,128]{4,3,2,1,0:T(8,128)(2,1)S(1)} %bitcast.142), kind=kOutput, calls=%fused_computation.33 | convolution fusion | flops 136314880 | bytes 7880704 | tf_op jit(solution)/shard_map/rqhkw,rkwhd->rqhd/dot_general | solution.py:152
  173.5 4.5 %convolution_convert_fusion = bf16[256,2048]{1,0:T(8,128)(2,1)} fusion(bf16[1024,2048]{1,0:T(8,128)(2,1)} %param.24, bf16[32,8,8,128]{3,2,1,0:T(8,128)(2,1)S(1)} %bitcast.149), kind=kOutput, calls=%fused_computation.17 | convolution fusion | flops 1074266112 | bytes 5767168 | tf_op jit(solution)/shard_map/dot_general | solution.py:160
  178.0 7.1 %reduce-scatter.2.cloned.1.call-done = bf16[128,2048]{1,0:T(8,128)(2,1)} async-done(((bf16[256,2048]{1,0:T(8,128)(2,1)}), bf16[128,2048]{1,0:T(8,128)(2,1)}) %reduce-scatter.2.cloned.1.call-update) | async-done | bytes 524304 | tf_op jit(solution)/shard_map/reduce_scatter | solution.py:159
  185.1 2.0 %fusion.40 = bf16[128,2048]{1,0:T(8,128)(2,1)} fusion(bf16[128,2048]{1,0:T(8,128)(2,1)S(1)} %copy-done.2, bf16[128,2048]{1,0:T(8,128)(2,1)} %reduce-scatter.2.cloned.1.call-done, f32[2048]{0:T(1024)S(1)} %bitcast.154), kind=kLoop, calls=%fused_computation.47 | loop fusion | flops 1310720 | bytes 1581056 | tf_op jit(solution)/shard_map/convert_element_type | solution.py:165
  (76 shorter events, 17.9 us)
Async XLA Ops:
  6.5 1.0 copy-start
  6.5 53.7 %copy-start.7 = (f32[2048]{0:T(1024)S(1)}, f32[2048]{0:T(1024)}, u32[]{:S(2)}) copy-start(f32[2048]{0:T(1024)} %param.17) | copy-start | bytes 24580
  6.5 53.7 %copy-start.6 = (bf16[64,2048]{1,0:T(8,128)(2,1)S(1)}, bf16[64,2048]{1,0:T(8,128)(2,1)}, u32[]{:S(2)}) copy-start(bf16[64,2048]{1,0:T(8,128)(2,1)} %param.14) | copy-start | bytes 786436
  6.5 72.0 %all-gather.3.cloned.1.call-start = ((), (), s32[]{:S(2)}) async-start(), calls=%async_computation.1 | async-start | bytes 1572864 | tf_op jit(solution)/shard_map/all_gather | solution.py:86
  55.6 100.6 %all-gather.5.cloned.1.call-start = ((), (), s32[]{:S(2)}) async-start(), calls=%async_computation.2 | async-start | bytes 4456448 | tf_op jit(solution)/shard_map/all_gather | solution.py:87
  55.7 4.6 %copy-start.3 = (bf16[2048,1024]{1,0:T(8,128)(2,1)S(1)}, bf16[2048,1024]{1,0:T(8,128)(2,1)}, u32[]{:S(2)}) copy-start(bf16[2048,1024]{1,0:T(8,128)(2,1)} %param.23) | copy-start | bytes 12582916
  56.9 5.0 %copy-start.8 = (f32[16,15,31]{2,0,1:T(8,128)S(1)}, f32[16,15,31]{2,0,1:T(8,128)}, u32[]{:S(2)}) copy-start(f32[16,15,31]{2,0,1:T(8,128)} %param.25) | copy-start | bytes 89284
  61.9 123.2 %reduce-scatter.2.cloned.1.call-start = ((), (), s32[]{:S(2)}) async-start(), calls=%async_computation.3 | async-start | bytes 1572864 | tf_op jit(solution)/shard_map/reduce_scatter | solution.py:159
  78.5 3.9 %copy-start.4 = (bf16[2048,1024]{1,0:T(8,128)(2,1)S(1)}, bf16[2048,1024]{1,0:T(8,128)(2,1)}, u32[]{:S(2)}) copy-start(bf16[2048,1024]{1,0:T(8,128)(2,1)} %param.22) | copy-start | bytes 12582916
  78.5 4.0 %copy-start.10 = (bf16[256,2048]{1,0:T(8,128)(2,1)S(1)}, bf16[256,2048]{1,0:T(8,128)(2,1)}, u32[]{:S(2)}) copy-start(bf16[256,2048]{1,0:T(8,128)(2,1)} %all-gather.3.cloned.1.call-done) | copy-start | bytes 3145732
  82.6 6.9 %copy-start.9 = (bf16[2048,1024]{1,0:T(8,128)(2,1)S(1)}, bf16[2048,1024]{1,0:T(8,128)(2,1)}, u32[]{:S(2)}) copy-start(bf16[2048,1024]{1,0:T(8,128)(2,1)} %param.21) | copy-start | bytes 12582916
  83.9 32.3 %collective-permute-start = (bf16[2,4,32,1024]{3,2,0,1:T(8,128)(2,1)S(1)}, bf16[2,4,32,1024]{3,2,0,1:T(8,128)(2,1)S(1)}, u32[]{:S(2)}, u32[]{:S(2)}) collective-permute-start(bf16[2,4,32,1024]{3,2,0,1:T(8,128)(2,1)S(1)} %get-tuple-element.9), channel_id=1, source_target_pairs={{0,2},{2,4},{4,6},{6,8},{8,10},{10,12},{12,14},{14,16},{16,18},{18... | collective-permute-start | bytes 1572872 | tf_op jit(solution)/shard_map/ppermute | solution.py:23
  88.2 30.0 %collective-permute-start.1 = (bf16[2,4,32,1024]{3,2,0,1:T(8,128)(2,1)S(1)}, bf16[2,4,32,1024]{3,2,0,1:T(8,128)(2,1)S(1)}, u32[]{:S(2)}, u32[]{:S(2)}) collective-permute-start(bf16[2,4,32,1024]{3,2,0,1:T(8,128)(2,1)S(1)} %get-tuple-element.10), channel_id=1, source_target_pairs={{2,0},{4,2},{6,4},{8,6},{10,8},{12,10},{14,12},{16,14},{18,16},{20... | collective-permute-start | bytes 1572872 | tf_op jit(solution)/shard_map/ppermute | solution.py:25
  127.3 4.5 %slice-start = ((s8[8388608]{0:T(1024)(128)(4,1)}), s8[4194304]{0:T(1024)(128)(4,1)S(1)}, s32[]{:S(2)}) async-start(s8[8388608]{0:T(1024)(128)(4,1)} %bitcast.132), calls=%async_computation.4 | async-start | bytes 8388608
  128.4 4.5 %slice-start.1 = ((s8[8388608]{0:T(1024)(128)(4,1)}), s8[4194304]{0:T(1024)(128)(4,1)S(1)}, s32[]{:S(2)}) async-start(s8[8388608]{0:T(1024)(128)(4,1)} %bitcast.132), calls=%async_computation.5 | async-start | bytes 8388608
  161.3 2.6 %slice-start.2 = ((s8[8388608]{0:T(1024)(128)(4,1)}), s8[4194304]{0:T(1024)(128)(4,1)S(1)}, s32[]{:S(2)}) async-start(s8[8388608]{0:T(1024)(128)(4,1)} %bitcast.134), calls=%async_computation.6 | async-start | bytes 8388608
  162.0 2.9 %slice-start.3 = ((s8[8388608]{0:T(1024)(128)(4,1)}), s8[4194304]{0:T(1024)(128)(4,1)S(1)}, s32[]{:S(2)}) async-start(s8[8388608]{0:T(1024)(128)(4,1)} %bitcast.134), calls=%async_computation.7 | async-start | bytes 8388608
  167.6 3.3 %copy-start.5 = (bf16[256,8,8,128]{3,2,1,0:T(8,128)(2,1)S(1)}, bf16[256,8,8,128]{3,2,1,0:T(8,128)(2,1)}, u32[]{:S(2)}) copy-start(bf16[256,8,8,128]{3,2,1,0:T(8,128)(2,1)} %copy.80) | copy-start | bytes 12582916
  173.5 11.7 %copy-start.2 = (bf16[128,2048]{1,0:T(8,128)(2,1)S(1)}, bf16[128,2048]{1,0:T(8,128)(2,1)}, u32[]{:S(2)}) copy-start(bf16[128,2048]{1,0:T(8,128)(2,1)} %param.13) | copy-start | bytes 1572868
  173.5 13.6 %copy-start.1 = (bf16[128,1024]{1,0:T(8,128)(2,1)S(1)}, bf16[128,1024]{1,0:T(8,128)(2,1)}, u32[]{:S(2)}) copy-start(bf16[128,1024]{1,0:T(8,128)(2,1)} %param.18) | copy-start | bytes 786436
Sparse Core Ops, SparseCore 0:
  55.7 8.8 all-gather.2
  67.3 88.8 all-gather.4
  178.1 6.9 reduce-scatter.1
where the time goes:
time: 194 us
  waiting for transfers between devices  53.3 us (27%)
  blocking collectives  42.3 us (22%)
  matrix products  35.6 us (18%)
  local copies, waits for them, and re-layouts  30 us (15%)
  between operations  13.6 us (7%)
  other arithmetic  13.3 us (7%)
  starting transfers between devices  5.61 us (3%)
    psum x1, blocking collectives, on_device(): mod_vecs = lax.psum(placed, ('sp', 'tp'))  42.3 us
    ppermute x1, waiting for transfers between devices, padded_2(): lax.ppermute(tail, axis, [(i, (i + 1) % count) for i in range(ends)])  25.2 us
    all_gather x1, waiting for transfers between devices, on_device(): lax.all_gather(project(rms_mod(context, norm_gain, mod_vecs[1], mod_vecs[...  19 us
    unnamed x36, local copies, waits for them, and re-layouts  11.5 us
    dot_general x5, matrix products, project(): jnp.dot(block, weight, preferred_element_type=jnp.float32)  10.6 us
    dot_general x1, local copies, waits for them, and re-layouts, on_device(): jnp.einsum('rke,heqw->rqhkw', row_hot, col_table, precision=lax.Precision...  9.27 us
    reduce_scatter x1, waiting for transfers between devices, on_device(): lax.psum_scatter(jnp.dot(attended, w_out, preferred_element_type=jnp.floa...  7.12 us
    dot_general x1, matrix products, on_device(): jnp.einsum('rke,heqw->rqhkw', row_hot, col_table, precision=lax.Precision...  5.61 us
  transfers between devices with their start and end apart: 5, of which 4 were waited for; matrix products, arithmetic and copies ran while one was open for 24% of the time, Pallas kernels for 0%

commit v1 on v0

--- a/solution.py
+++ b/solution.py
@@ -81,7 +81,7 @@
     placed = lax.dynamic_update_slice_in_dim(
         jnp.zeros((5, model_width), jnp.float32), partial_value, lax.axis_index("tp") * col_part, 1
     )
-    mod_vecs = lax.psum(placed, ("sp", "tp"))
+    mod_vecs = lax.psum(lax.psum(placed, "sp"), "tp")
     normed = rms_mod(latent, norm_gain, mod_vecs[0], mod_vecs[2])
     projected = project(lax.all_gather(normed, "tp", axis=0, tiled=True), (w_query, w_key, w_value))
     ctx_kv = lax.all_gather(

time: 194 us -> 230 us (1.19)
  blocking collectives: 42.3 us -> 82.2 us
  starting transfers between devices: 5.61 us -> 2.7 us
    psum x1 -> x2, blocking collectives: 42.3 us -> 82.2 us  [on_device(): mod_vecs = lax.psum(lax.psum(placed, 'sp'), 'tp')]
    ppermute x1, starting transfers between devices: 4.23 us -> 1.32 us  [padded_2(): lax.ppermute(tail, axis, [(i, (i + 1) % count) for i in range(ends)])]
    ppermute x1, waiting for transfers between devices: 25.2 us -> 27.7 us  [padded_2(): lax.ppermute(tail, axis, [(i, (i + 1) % count) for i in range(ends)])]
  transfers between devices with their start and end apart: 5 -> 5, of which waited for: 4 -> 3; matrix products, arithmetic and copies ran while one was open for 24% -> 21% of each run, Pallas kernels for 0% -> 0%
where the time goes in v1:
time: 230 us
  blocking collectives  82.2 us (36%)
  waiting for transfers between devices  52.7 us (23%)
  matrix products  36 us (16%)
  local copies, waits for them, and re-layouts  29.1 us (13%)
  between operations  13.6 us (6%)
  other arithmetic  13.3 us (6%)
  starting transfers between devices  2.7 us (1%)
    psum x2, blocking collectives, on_device(): mod_vecs = lax.psum(lax.psum(placed, 'sp'), 'tp')  82.2 us
    ppermute x1, waiting for transfers between devices, padded_2(): lax.ppermute(tail, axis, [(i, (i + 1) % count) for i in range(ends)])  27.7 us
    all_gather x1, waiting for transfers between devices, on_device(): lax.all_gather(project(rms_mod(context, norm_gain, mod_vecs[1], mod_vecs[...  17.8 us
    dot_general x5, matrix products, project(): jnp.dot(block, weight, preferred_element_type=jnp.float32)  10.9 us
    unnamed x36, local copies, waits for them, and re-layouts  10.1 us
    dot_general x1, local copies, waits for them, and re-layouts, on_device(): jnp.einsum('rke,heqw->rqhkw', row_hot, col_table, precision=lax.Precision...  9.27 us
    reduce_scatter x1, waiting for transfers between devices, on_device(): lax.psum_scatter(jnp.dot(attended, w_out, preferred_element_type=jnp.floa...  7.12 us
    dot_general x1, matrix products, on_device(): jnp.einsum('rke,heqw->rqhkw', row_hot, col_table, precision=lax.Precision...  5.63 us
  transfers between devices with their start and end apart: 5, of which 3 were waited for; matrix products, arithmetic and copies ran while one was open for 21% of the time, Pallas kernels for 0%

profile of v1, /device:TPU:0, one launch (start us, length us, event | category | flops | bytes accessed | tf_op | source)
XLA Modules:
  0.0 229.7 jit_solution(7250962571477158795)
XLA Ops:
  9.9 78.7 %psum.14 = f32[5,2048]{1,0:T(8,128)S(1)} all-reduce(f32[5,2048]{1,0:T(8,128)S(1)} %maximum_dynamic-update-slice_fusion), channel_id=1, replica_groups=mesh['sp'=16,'tp'=2] {'sp'}, use_global_device_ids=true, to_apply=%region_0.1 | all-reduce | flops 10240 | bytes 81920 | tf_op jit(solution)/shard_map/psum | solution.py:84
  88.6 3.6 %psum.15 = f32[5,2048]{1,0:T(8,128)S(1)} all-reduce(f32[5,2048]{1,0:T(8,128)S(1)} %psum.14), channel_id=1, replica_groups=mesh['sp'=16,'tp'=2] {'tp'}, use_global_device_ids=true, to_apply=%region_1.2 | all-reduce | flops 10240 | bytes 81920 | tf_op jit(solution)/shard_map/psum | solution.py:84
  93.4 2.1 fusion.39
  96.9 3.6 %fusion.33 = bf16[1,64,1024]{2,1,0:T(8,128)(2,1)S(1)} fusion(bf16[2048,1024]{1,0:T(8,128)(2,1)} %param.22, bf16[64,2048]{1,0:T(8,128)(2,1)} %param.14, f32[2048]{0:T(1024)S(1)} %bitcast.150, f32[2048]{0:T(1024)S(1)} %bitcast.152, f32[2048]{0:T(1024)} %param.17, f32[64]{0:T(128)S(1)} %add_rsqrt_fusion), kind=kOutput, calls=%fused_computation.40 | convolution fusion | flops 269287424 | bytes 4612352 | tf_op jit(solution)/shard_map/dot_general | solution.py:43
  102.4 1.4 fusion.51
  103.8 5.6 %fusion.12 = f32[8,32,32,8,8]{2,4,3,1,0:T(8,128)} fusion(f32[8,15,32,32]{3,1,2,0:T(8,128)S(1)} %fusion.51, s32[8,8]{1,0:T(8,128)S(1)} %subtract_add_fusion), kind=kOutput, calls=%fused_computation.21 | convolution fusion | flops 94372800 | bytes 2588928 | tf_op jit(solution)/shard_map/rke,heqw->rqhkw/dot_general | solution.py:132
  109.5 9.3 %copy.59 = f32[8,32,32,8,8]{1,2,4,0,3:T(8,128)} copy(f32[8,32,32,8,8]{2,4,3,1,0:T(8,128)} %fusion.12) | data formatting | bytes 4194304 | tf_op jit(solution)/shard_map/rke,heqw->rqhkw/dot_general | solution.py:132
  118.8 3.9 %convolution_convert_fusion.2 = bf16[256,1024]{1,0:T(8,128)(2,1)S(1)} fusion(bf16[256,2048]{1,0:T(8,128)(2,1)} %all-gather.3.cloned.1.call-done, bf16[2048,1024]{1,0:T(8,128)(2,1)} %param.23), kind=kOutput, calls=%fused_computation.35 | convolution fusion | flops 1074003968 | bytes 5767168 | tf_op jit(solution)/shard_map/dot_general | solution.py:43
  124.2 1.3 collective-permute-start
  125.6 1.3 collective-permute-start.1
  128.4 27.7 %collective-permute-done = bf16[2,4,32,1024]{3,2,0,1:T(8,128)(2,1)S(1)} collective-permute-done((bf16[2,4,32,1024]{3,2,0,1:T(8,128)(2,1)S(1)}, bf16[2,4,32,1024]{3,2,0,1:T(8,128)(2,1)S(1)}, u32[]{:S(2)}, u32[]{:S(2)}) %collective-permute-start) | collective-permute-done | bytes 524320 | tf_op jit(solution)/shard_map/ppermute | solution.py:23
  156.4 4.9 %gather_fusion = bf16[8,2,8,32,1024]{4,3,1,2,0:T(8,128)(2,1)} fusion(bf16[2,16,32,1024]{3,2,0,1:T(8,128)(2,1)S(1)} %pad_maximum_fusion, s32[8]{0:T(128)S(1)} %shift-left_bitcast_fusion), kind=kCustom, calls=%fused_computation | custom fusion | bytes 16777344 | tf_op jit(solution)/shard_map/vmap()/gather | solution.py:109
  161.3 4.5 %fusion.66 = (bf16[8,1,8,32,1024]{4,3,1,2,0:T(8,128)(2,1)S(1)}, bf16[8,1,8,32,1024]{4,3,1,2,0:T(8,128)(2,1)S(1)}) fusion(bf16[8,2,8,32,1024]{4,3,1,2,0:T(8,128)(2,1)} %gather_fusion), kind=kLoop, calls=%fused_computation.99 | loop fusion | bytes 16777216 | tf_op jit(solution)/shard_map/slice | solution.py:113
  167.0 3.1 %copy.80 = bf16[256,8,8,128]{3,2,1,0:T(8,128)(2,1)} copy(bf16[256,8,8,128]{3,1,2,0:T(8,128)(2,1)S(1)} %bitcast.137) | data formatting | bytes 8388608
  170.1 4.3 %fusion.68 = (f32[8,32,8]{1,2,0:T(8,128)S(1)}, f32[8,32,8,8,32]{1,4,3,2,0:T(8,128)}) fusion(f32[8,32,32,8,8]{1,2,4,0,3:T(8,128)S(1)} %bitcast.133, bf16[8,32,8,128,1]{3,2,1,0,4:T(8,128)(2,1)S(1)} %bitcast_bitcast_fusion, bf16[8,8,32,8,128]{4,3,2,1,0:T(8,128)(2,1)S(1)} %bitcast.136, pred[32,32]{0,1:T(8,128)(4,1)S(1)} %fusion.57), kind=kOutput, calls=%fused_computation.101 | convolution fusion | flops 136312832 | bytes 8922112 | tf_op jit(solution)/shard_map/rqhd,rkwhd->rqhkw/dot_general | solution.py:135
  174.4 17.8 %all-gather.5.cloned.1.call-done = bf16[2,1024,1024]{2,1,0:T(8,128)(2,1)} async-done(((bf16[2,64,1024]{2,1,0:T(8,128)(2,1)}), bf16[2,1024,1024]{2,1,0:T(8,128)(2,1)}) %all-gather.5.cloned.1.call-update) | async-done | bytes 4194320 | tf_op jit(solution)/shard_map/all_gather | solution.py:87
  192.2 3.2 %slice_bitcast_fusion = (bf16[128,8,8,128]{3,1,2,0:T(8,128)(2,1)S(1)}, bf16[128,8,8,128]{3,1,2,0:T(8,128)(2,1)S(1)}) fusion(bf16[2,1024,1024]{2,1,0:T(8,128)(2,1)} %all-gather.5.cloned.1.call-done), kind=kLoop, calls=%fused_computation.18 | loop fusion | bytes 8388608
  198.1 1.9 fusion.3
  201.0 2.0 fusion.2
  203.7 3.3 %fusion.21 = f32[8,32,8,128]{3,1,2,0:T(8,128)S(1)} fusion(bf16[1024,8,128]{2,1,0:T(8,128)(2,1)S(1)} %bitcast.143, f32[8,32,8]{1,0,2:T(8,128)S(1)} %copy.67, f32[8,32,8]{1,0,2:T(8,128)S(1)} %copy.63, f32[8,1024,256]{1,2,0:S(1)} %fusion.16), kind=kOutput, calls=%fused_computation.31 | convolution fusion | flops 545259520 | bytes 11550720 | tf_op jit(solution)/shard_map/rqhc,chd->rqhd/dot_general | solution.py:155
  207.0 2.3 %fusion.29 = bf16[8,32,8,128]{3,1,2,0:T(8,128)(2,1)S(1)} fusion(f32[8,32,8,128]{3,1,2,0:T(8,128)S(1)} %fusion.21, f32[8,32,8,8,32]{1,4,3,2,0:T(8,128)S(1)} %bitcast.135, f32[8,32,8]{1,2,0:T(8,128)S(1)} %copy_add_fusion, f32[8,32,8]{1,2,0:T(8,128)S(1)} %copy_maximum_fusion, bf16[8,8,32,8,128]{4,3,2,1,0:T(8,128)(2,1)S(1)} %bitcast.142), kind=kOutput, calls=%fused_computation.33 | convolution fusion | flops 136314880 | bytes 7880704 | tf_op jit(solution)/shard_map/rqhkw,rkwhd->rqhd/dot_general | solution.py:152
  209.5 4.5 %convolution_convert_fusion = bf16[256,2048]{1,0:T(8,128)(2,1)} fusion(bf16[1024,2048]{1,0:T(8,128)(2,1)} %param.24, bf16[32,8,8,128]{3,2,1,0:T(8,128)(2,1)S(1)} %bitcast.149), kind=kOutput, calls=%fused_computation.17 | convolution fusion | flops 1074266112 | bytes 5767168 | tf_op jit(solution)/shard_map/dot_general | solution.py:160
  214.0 7.1 %reduce-scatter.2.cloned.1.call-done = bf16[128,2048]{1,0:T(8,128)(2,1)} async-done(((bf16[256,2048]{1,0:T(8,128)(2,1)}), bf16[128,2048]{1,0:T(8,128)(2,1)}) %reduce-scatter.2.cloned.1.call-update) | async-done | bytes 524304 | tf_op jit(solution)/shard_map/reduce_scatter | solution.py:159
  221.2 2.0 fusion.40
  (77 shorter events, 16.7 us)
Async XLA Ops:
  6.5 1.0 copy-start
  6.5 93.9 %copy-start.7 = (f32[2048]{0:T(1024)S(1)}, f32[2048]{0:T(1024)}, u32[]{:S(2)}) copy-start(f32[2048]{0:T(1024)} %param.17) | copy-start | bytes 24580
  6.5 94.0 %copy-start.6 = (bf16[64,2048]{1,0:T(8,128)(2,1)S(1)}, bf16[64,2048]{1,0:T(8,128)(2,1)}, u32[]{:S(2)}) copy-start(bf16[64,2048]{1,0:T(8,128)(2,1)} %param.14) | copy-start | bytes 786436
  6.5 112.3 %all-gather.3.cloned.1.call-start = ((), (), s32[]{:S(2)}) async-start(), calls=%async_computation.1 | async-start | bytes 1572864 | tf_op jit(solution)/shard_map/all_gather | solution.py:86
  95.6 96.7 %all-gather.5.cloned.1.call-start = ((), (), s32[]{:S(2)}) async-start(), calls=%async_computation.2 | async-start | bytes 4456448 | tf_op jit(solution)/shard_map/all_gather | solution.py:87
  95.6 4.9 %copy-start.3 = (bf16[2048,1024]{1,0:T(8,128)(2,1)S(1)}, bf16[2048,1024]{1,0:T(8,128)(2,1)}, u32[]{:S(2)}) copy-start(bf16[2048,1024]{1,0:T(8,128)(2,1)} %param.23) | copy-start | bytes 12582916
  96.9 5.4 %copy-start.8 = (f32[16,15,31]{2,0,1:T(8,128)S(1)}, f32[16,15,31]{2,0,1:T(8,128)}, u32[]{:S(2)}) copy-start(f32[16,15,31]{2,0,1:T(8,128)} %param.25) | copy-start | bytes 89284
  102.2 119.0 %reduce-scatter.2.cloned.1.call-start = ((), (), s32[]{:S(2)}) async-start(), calls=%async_computation.3 | async-start | bytes 1572864 | tf_op jit(solution)/shard_map/reduce_scatter | solution.py:159
  118.8 3.9 %copy-start.4 = (bf16[2048,1024]{1,0:T(8,128)(2,1)S(1)}, bf16[2048,1024]{1,0:T(8,128)(2,1)}, u32[]{:S(2)}) copy-start(bf16[2048,1024]{1,0:T(8,128)(2,1)} %param.22) | copy-start | bytes 12582916
  118.8 4.0 %copy-start.10 = (bf16[256,2048]{1,0:T(8,128)(2,1)S(1)}, bf16[256,2048]{1,0:T(8,128)(2,1)}, u32[]{:S(2)}) copy-start(bf16[256,2048]{1,0:T(8,128)(2,1)} %all-gather.3.cloned.1.call-done) | copy-start | bytes 3145732
  122.9 4.0 %copy-start.9 = (bf16[2048,1024]{1,0:T(8,128)(2,1)S(1)}, bf16[2048,1024]{1,0:T(8,128)(2,1)}, u32[]{:S(2)}) copy-start(bf16[2048,1024]{1,0:T(8,128)(2,1)} %param.21) | copy-start | bytes 12582916
  124.2 31.9 %collective-permute-start = (bf16[2,4,32,1024]{3,2,0,1:T(8,128)(2,1)S(1)}, bf16[2,4,32,1024]{3,2,0,1:T(8,128)(2,1)S(1)}, u32[]{:S(2)}, u32[]{:S(2)}) collective-permute-start(bf16[2,4,32,1024]{3,2,0,1:T(8,128)(2,1)S(1)} %get-tuple-element.9), channel_id=1, source_target_pairs={{0,2},{2,4},{4,6},{6,8},{8,10},{10,12},{12,14},{14,16},{16,18},{18... | collective-permute-start | bytes 1572872 | tf_op jit(solution)/shard_map/ppermute | solution.py:23
  125.6 30.6 %collective-permute-start.1 = (bf16[2,4,32,1024]{3,2,0,1:T(8,128)(2,1)S(1)}, bf16[2,4,32,1024]{3,2,0,1:T(8,128)(2,1)S(1)}, u32[]{:S(2)}, u32[]{:S(2)}) collective-permute-start(bf16[2,4,32,1024]{3,2,0,1:T(8,128)(2,1)S(1)} %get-tuple-element.10), channel_id=1, source_target_pairs={{2,0},{4,2},{6,4},{8,6},{10,8},{12,10},{14,12},{16,14},{18,16},{20... | collective-permute-start | bytes 1572872 | tf_op jit(solution)/shard_map/ppermute | solution.py:25
  165.8 4.3 %slice-start = ((s8[8388608]{0:T(1024)(128)(4,1)}), s8[4194304]{0:T(1024)(128)(4,1)S(1)}, s32[]{:S(2)}) async-start(s8[8388608]{0:T(1024)(128)(4,1)} %bitcast.132), calls=%async_computation.4 | async-start | bytes 8388608
  166.9 3.1 %slice-start.1 = ((s8[8388608]{0:T(1024)(128)(4,1)}), s8[4194304]{0:T(1024)(128)(4,1)S(1)}, s32[]{:S(2)}) async-start(s8[8388608]{0:T(1024)(128)(4,1)} %bitcast.132), calls=%async_computation.5 | async-start | bytes 8388608
  197.3 2.6 %slice-start.2 = ((s8[8388608]{0:T(1024)(128)(4,1)}), s8[4194304]{0:T(1024)(128)(4,1)S(1)}, s32[]{:S(2)}) async-start(s8[8388608]{0:T(1024)(128)(4,1)} %bitcast.134), calls=%async_computation.6 | async-start | bytes 8388608
  198.1 2.9 %slice-start.3 = ((s8[8388608]{0:T(1024)(128)(4,1)}), s8[4194304]{0:T(1024)(128)(4,1)S(1)}, s32[]{:S(2)}) async-start(s8[8388608]{0:T(1024)(128)(4,1)} %bitcast.134), calls=%async_computation.7 | async-start | bytes 8388608
  203.7 3.3 %copy-start.5 = (bf16[256,8,8,128]{3,2,1,0:T(8,128)(2,1)S(1)}, bf16[256,8,8,128]{3,2,1,0:T(8,128)(2,1)}, u32[]{:S(2)}) copy-start(bf16[256,8,8,128]{3,2,1,0:T(8,128)(2,1)} %copy.80) | copy-start | bytes 12582916
  209.5 11.7 %copy-start.2 = (bf16[128,2048]{1,0:T(8,128)(2,1)S(1)}, bf16[128,2048]{1,0:T(8,128)(2,1)}, u32[]{:S(2)}) copy-start(bf16[128,2048]{1,0:T(8,128)(2,1)} %param.13) | copy-start | bytes 1572868
  209.5 13.6 %copy-start.1 = (bf16[128,1024]{1,0:T(8,128)(2,1)S(1)}, bf16[128,1024]{1,0:T(8,128)(2,1)}, u32[]{:S(2)}) copy-start(bf16[128,1024]{1,0:T(8,128)(2,1)} %param.18) | copy-start | bytes 786436
Sparse Core Ops, SparseCore 0:
  95.7 5.1 all-gather.2
  103.6 88.6 all-gather.4
  214.2 6.9 reduce-scatter.1
